TPU v7x, 256 devices: a whole 4x4x8 slice. The times are simulated.
256 devices in a mesh: sp: 32 (over z, y), tp: 8 (over x, core).
Axes of the slice: x: 4, y: 4, z: 8, core: 2. Of those that a mesh axis runs over, the one named last changes fastest.
Arguments:
- hidden: bfloat16 [24576, 2048], P(('sp', 'tp')), may hold values from -6 to 6
- norm_gain: float32 [2, 2048], replicated, may hold values from 0.1 to 1.9
- w_value: bfloat16 [2, 2048, 2048], P(None, 'sp', 'tp'), may hold values from -0.125 to 0.125
- w_gate: bfloat16 [2, 2048, 2048], P(None, 'sp', 'tp'), may hold values from -0.125 to 0.125
- conv_weight: float32 [2, 31, 2048], P(None, None, 'tp'), may hold values from -3 to 3
- conv_bias: float32 [2, 2048], P(None, 'tp'), may hold values from -3 to 3
- chan_gain: float32 [2, 2048], P(None, 'tp'), may hold values from 0.1 to 1.9
- chan_shift: float32 [2, 2048], P(None, 'tp'), may hold values from -3 to 3
- w_out: bfloat16 [2, 2048, 2048], P(None, 'tp', 'sp'), may hold values from -0.125 to 0.125
Outputs:
- result: bfloat16 [24576, 2048], P(('sp', 'tp'))
All inputs are finite; a program needn't handle non-finite values.
Results may differ from a plain program's by a relative error of at most 0.015.
Values may be sent and summed in bfloat16 or wider, within the bound.
No kernel may reach another device: no remote copies, remote signals or barrier semaphores. Data moves between devices by JAX's collectives and lax.ppermute only.
A program may use at most 64 MiB of HBM per device.

v0:
```python
import jax
import jax.numpy as jnp
from jax import lax
from jax.sharding import Mesh
from jax.sharding import PartitionSpec as P

SP = ("sp_0", "sp_1")
SP_TP = ("sp_0", "sp_1", "tp")
EPS = 1e-06


def sent_together(arrays, axis, dim, along):
    widths = [a.shape[along] for a in arrays]
    both = jnp.concatenate(arrays, axis=along)
    whole = lax.all_gather(both, axis, axis=dim, tiled=True)
    return tuple(jnp.split(whole, [sum(widths[:k]) for k in range(1, len(widths))], axis=along))


def shifted(shard, axis, by):
    size = lax.axis_size(axis)
    pairs = [(i, i + by) for i in range(size) if 0 <= i + by < size]
    return lax.ppermute(shard, axis, pairs)


def sent_to_all(shard, axis):
    size = lax.axis_size(axis)
    return lax.all_to_all(
        jnp.broadcast_to(shard[None], (size, *shard.shape)), axis, 0, 0, tiled=True
    )


def of_everyone(shard, axis):
    everything = sent_to_all(shard, axis)
    return jnp.sum(everything, axis=0)


def together(arrays, axis):
    ravelled, at, finished = (jnp.concatenate([a.reshape(-1) for a in arrays]), 0, [])
    running = of_everyone(ravelled, axis)
    for a in arrays:
        finished.append(running[at : at + a.size].reshape(a.shape))
        at += a.size
    return tuple(finished)


def whole_of(shard, axes, dim):
    if not axes:
        return shard
    nearer = lax.all_gather(shard, axes[-1], axis=dim, tiled=True)
    return whole_of(nearer, axes[:-1], dim)


def cut_along(shard, dim, size):
    dims = shard.shape
    tiles = shard.reshape(*dims[:dim], size, dims[dim] // size, *dims[dim + 1 :])
    return jnp.moveaxis(tiles, dim, 0)


def sum_at_owner(shard, axis, dim):
    tiles = cut_along(shard, dim, lax.axis_size(axis))
    arrived = lax.all_to_all(tiles, axis, split_axis=0, concat_axis=0, tiled=True)
    return arrived.astype(jnp.float32).sum(axis=0)


def body(hidden, norm_gain, w_value, w_gate, conv_weight, conv_bias, chan_gain, chan_shift, w_out):
    group = lax.axis_size("tp")
    own_rows = hidden.shape[0]
    chans = w_value.shape[2]
    taps = conv_weight.shape[1]
    state = hidden
    for layer in range(norm_gain.shape[0]):
        xf = state.astype(jnp.float32)
        scale = lax.rsqrt(jnp.mean(xf * xf, axis=1, keepdims=True) + EPS)
        normed = (xf * scale * norm_gain[layer][None, :]).astype(jnp.bfloat16)
        tokens = lax.all_gather(normed, "tp", axis=0, tiled=True)
        empty = jnp.zeros((tokens.shape[0], chans), jnp.float32)

        def add_both(totals, pieces, start, tokens=tokens):
            return (
                jnp.dot(tokens, pieces[0], preferred_element_type=jnp.float32),
                jnp.dot(tokens, pieces[1], preferred_element_type=jnp.float32),
            )

        lin, gate = add_both(
            (empty, empty), sent_together((w_value[layer], w_gate[layer]), SP, 0, 1), jnp.int32(0)
        )
        glu = (lin * jax.nn.sigmoid(gate)).astype(jnp.bfloat16)
        before = shifted(glu[tokens.shape[0] - (taps - 1) :], SP, 1)
        window = jnp.concatenate([before, glu], axis=0).astype(jnp.float32)
        length = tokens.shape[0]
        mixed = jnp.zeros((length, chans), jnp.float32) + conv_bias[layer][None, :]
        for tap in range(taps):
            mixed = mixed + conv_weight[layer, tap][None, :] * window[tap : tap + length]
        totals = together((jnp.sum(mixed, axis=1), jnp.sum(mixed * mixed, axis=1)), "tp")
        mean = (totals[0] / (chans * group))[:, None]
        msq = (totals[1] / (chans * group))[:, None]
        var = msq - mean * mean
        act = jax.nn.silu(
            (mixed - mean) * lax.rsqrt(var + EPS) * chan_gain[layer][None, :]
            + chan_shift[layer][None, :]
        ).astype(jnp.bfloat16)

        def project(piece, start, act=act):
            return jnp.dot(act, piece, preferred_element_type=jnp.float32)

        partial_out = project(whole_of(w_out[layer], SP, 1), jnp.int32(0))

        def take_rows(start, count, partial_out=partial_out):
            return partial_out

        update = sum_at_owner(
            take_rows(jnp.int32(0), own_rows * lax.axis_size("tp")).astype(jnp.bfloat16), "tp", 0
        )
        state = (xf + update).astype(jnp.bfloat16)
    return state


def solution(mesh):
    torus = Mesh(mesh.devices.reshape(8, 4, mesh.shape["tp"]), ("sp_0", "sp_1", "tp"))
    in_specs = (
        P(SP_TP, None),
        P(),
        P(None, SP, "tp"),
        P(None, SP, "tp"),
        P(None, None, "tp"),
        P(None, "tp"),
        P(None, "tp"),
        P(None, "tp"),
        P(None, "tp", SP),
    )
    out_specs = P(SP_TP, None)
    return jax.shard_map(body, mesh=torus, in_specs=in_specs, out_specs=out_specs, check_vma=False)
```

profile of v0, /device:TPU:1, one launch (start us, length us, event | category | flops | bytes accessed | tf_op | source)
XLA Modules:
  0.0 361.9 jit_solution(7405386278213270947)
XLA Ops:
  6.5 0.8 slice_bitcast_fusion
  7.4 0.6 pad_maximum_fusion
  8.0 0.0 all-gather.11.cloned.1.call-start
  8.1 1.2 fusion.14
  9.2 0.8 fusion.112
  10.1 1.9 fusion.16
  12.0 0.0 all-gather.19.cloned.1.call-start
  12.0 0.8 fusion.107
  12.8 11.2 %all-gather = bf16[1,256,256]{1,2,0:T(8,128)(2,1)} all-gather(bf16[1,256,64]{1,2,0:T(8,128)(2,1)S(1)} %get-tuple-element.17), channel_id=2, replica_groups=mesh['sp_0'=8,'sp_1'=4,'tp'=8] {'sp_1'}, dimensions={2}, use_global_device_ids=true | all-gather | bytes 163840 | tf_op jit(solution)/shard_map/all_gather | solution.py:49
  24.0 0.0 all-gather.17.cloned.1.call-start
  24.1 0.6 pad_maximum_fusion.1
  24.7 0.9 fusion.110
  25.6 0.9 fusion.109
  26.5 0.8 fusion.111
  27.3 0.8 fusion.115
  28.0 59.0 %all-gather.13.cloned.1.call-done = bf16[2048,512]{1,0:T(8,128)(2,1)} async-done(((bf16[64,512]{1,0:T(8,128)(2,1)}), bf16[2048,512]{1,0:T(8,128)(2,1)}) %all-gather.13.cloned.1.call-update) | async-done | bytes 2097168 | tf_op jit(solution)/shard_map/all_gather | solution.py:15
  87.1 34.3 %all-gather.11.cloned.1.call-done = bf16[768,2048]{1,0:T(8,128)(2,1)} async-done(((bf16[96,2048]{1,0:T(8,128)(2,1)}), bf16[768,2048]{1,0:T(8,128)(2,1)}) %all-gather.11.cloned.1.call-update) | async-done | bytes 3145744 | tf_op jit(solution)/shard_map/all_gather | solution.py:75
  121.4 3.3 fusion.3
  124.7 1.0 fusion.6
  125.8 3.1 collective-permute-start
  128.9 0.8 collective-permute-done
  129.7 0.1 maximum_convert_fusion
  129.8 3.5 fusion.103
  133.4 0.6 broadcast_in_dim.4
  134.0 4.4 %all-to-all-start = ((f32[8,1,1536]{2,1,0:T(1,128)}), f32[8,1,1536]{2,1,0:T(1,128)S(1)}, u32[]{:S(2)}, u32[]{:S(2)}) async-start(f32[8,1,1536]{2,1,0:T(1,128)} %broadcast_in_dim.4), calls=%async_computation | async-start | bytes 98304 | tf_op jit(solution)/shard_map/all_to_all | solution.py:27
  138.4 4.8 %all-to-all-done = f32[8,1,1536]{2,1,0:T(1,128)S(1)} async-done(((f32[8,1,1536]{2,1,0:T(1,128)}), f32[8,1,1536]{2,1,0:T(1,128)S(1)}, u32[]{:S(2)}, u32[]{:S(2)}) %all-to-all-start) | async-done | bytes 49184 | tf_op jit(solution)/shard_map/all_to_all | solution.py:27
  143.3 13.7 %all-gather.19.cloned.1.call-done = bf16[1,256,2048]{1,2,0:T(8,128)(2,1)} async-done(((bf16[1,256,256]{1,2,0:T(8,128)(2,1)}), bf16[1,256,2048]{1,2,0:T(8,128)(2,1)}) %all-gather.19.cloned.1.call-update) | async-done | bytes 1048592 | tf_op jit(solution)/shard_map/all_gather | solution.py:49
  156.9 2.3 convolution_convert_fusion.1
  159.3 46.4 %all_to_all.22 = bf16[8,96,2048]{2,1,0:T(8,128)(2,1)S(1)} all-to-all(bf16[8,96,2048]{2,1,0:T(8,128)(2,1)S(1)} %bitcast.90), channel_id=1, replica_groups=mesh['sp_0'=8,'sp_1'=4,'tp'=8] {'tp'}, dimensions={0} | all-to-all | bytes 6291456 | tf_op jit(solution)/shard_map/all_to_all | solution.py:61
  205.7 0.6 convert_reduce_fusion.1
  206.3 0.4 copy-done
  206.7 0.2 fusion.18
  206.9 0.9 fusion.20
  207.9 11.0 %all-gather.2 = bf16[1,256,256]{1,2,0:T(8,128)(2,1)} all-gather(bf16[1,256,64]{1,2,0:T(8,128)(2,1)S(1)} %get-tuple-element.18), channel_id=4, replica_groups=mesh['sp_0'=8,'sp_1'=4,'tp'=8] {'sp_1'}, dimensions={2}, use_global_device_ids=true | all-gather | bytes 163840 | tf_op jit(solution)/shard_map/all_gather | solution.py:49
  219.0 16.4 %all-gather.17.cloned.1.call-done = bf16[2048,512]{1,0:T(8,128)(2,1)} async-done(((bf16[64,512]{1,0:T(8,128)(2,1)}), bf16[2048,512]{1,0:T(8,128)(2,1)}) %all-gather.17.cloned.1.call-update) | async-done | bytes 2097168 | tf_op jit(solution)/shard_map/all_gather | solution.py:15
  235.4 34.2 %all-gather.15.cloned.1.call-done = bf16[768,2048]{1,0:T(8,128)(2,1)} async-done(((bf16[96,2048]{1,0:T(8,128)(2,1)}), bf16[768,2048]{1,0:T(8,128)(2,1)}) %all-gather.15.cloned.1.call-update) | async-done | bytes 3145744 | tf_op jit(solution)/shard_map/all_gather | solution.py:75
  269.6 3.3 fusion.5
  272.9 1.0 fusion.7
  273.9 3.1 collective-permute-start.1
  277.0 0.9 fusion.108
  277.9 0.1 maximum_convert_fusion.1
  278.0 3.5 fusion.102
  281.6 8.6 %all_to_all.23 = f32[8,1,1536]{2,1,0:T(1,128)S(1)} all-to-all(f32[8,1,1536]{2,1,0:T(1,128)S(1)} %broadcast_in_dim.5), channel_id=1, replica_groups=mesh['sp_0'=8,'sp_1'=4,'tp'=8] {'tp'}, dimensions={0} | all-to-all | bytes 98304 | tf_op jit(solution)/shard_map/all_to_all | solution.py:27
  290.3 13.9 %all-gather.21.cloned.1.call-done = bf16[1,256,2048]{1,2,0:T(8,128)(2,1)} async-done(((bf16[1,256,256]{1,2,0:T(8,128)(2,1)}), bf16[1,256,2048]{1,2,0:T(8,128)(2,1)}) %all-gather.21.cloned.1.call-update) | async-done | bytes 1048592 | tf_op jit(solution)/shard_map/all_gather | solution.py:49
  304.2 2.3 convolution_convert_fusion
  306.5 47.1 %all_to_all.24 = bf16[8,96,2048]{2,1,0:T(8,128)(2,1)S(1)} all-to-all(bf16[8,96,2048]{2,1,0:T(8,128)(2,1)S(1)} %bitcast.91), channel_id=1, replica_groups=mesh['sp_0'=8,'sp_1'=4,'tp'=8] {'tp'}, dimensions={0} | all-to-all | bytes 6291456 | tf_op jit(solution)/shard_map/all_to_all | solution.py:61
  353.7 0.6 convert_reduce_fusion
  354.2 0.8 fusion.21
  (36 shorter events, 0.4 us)
Async XLA Ops:
  6.5 80.5 %all-gather.13.cloned.1.call-start = ((), (), s32[]{:S(2)}) async-start(), calls=%async_computation.5 | async-start | bytes 2162688 | tf_op jit(solution)/shard_map/all_gather | solution.py:15
  8.0 113.4 %all-gather.11.cloned.1.call-start = ((), (), s32[]{:S(2)}) async-start(), calls=%async_computation.4 | async-start | bytes 3538944 | tf_op jit(solution)/shard_map/all_gather | solution.py:75
  12.0 144.9 %all-gather.19.cloned.1.call-start = ((), (), s32[]{:S(2)}) async-start(), calls=%async_computation.8 | async-start | bytes 1179648 | tf_op jit(solution)/shard_map/all_gather | solution.py:49
  24.0 211.3 %all-gather.17.cloned.1.call-start = ((), (), s32[]{:S(2)}) async-start(), calls=%async_computation.7 | async-start | bytes 2162688 | tf_op jit(solution)/shard_map/all_gather | solution.py:15
  87.1 37.6 %copy-start.6 = (bf16[2048,512]{1,0:T(8,128)(2,1)S(1)}, bf16[2048,512]{1,0:T(8,128)(2,1)}, u32[]{:S(2)}) copy-start(bf16[2048,512]{1,0:T(8,128)(2,1)} %all-gather.13.cloned.1.call-done) | copy-start | bytes 6291460
  121.4 3.3 copy-start.3
  124.7 4.2 %copy-start.1 = (f32[2,256]{1,0:T(2,128)S(1)}, f32[2,256]{1,0:T(2,128)}, u32[]{:S(2)}) copy-start(f32[2,256]{1,0:T(2,128)} %param.15) | copy-start | bytes 6148
  125.8 4.0 %collective-permute-start = (bf16[30,256]{1,0:T(8,128)(2,1)S(1)}, bf16[30,256]{1,0:T(8,128)(2,1)S(1)}, u32[]{:S(2)}, u32[]{:S(2)}) collective-permute-start(bf16[30,256]{1,0:T(8,128)(2,1)S(1)} %slice.576), channel_id=1, source_target_pairs={{0,8},{8,16},{16,24},{24,32},{32,40},{40,48},{48,56},{56,64},{64,7... | collective-permute-start | bytes 46088 | tf_op jit(solution)/shard_map/ppermute | solution.py:22
  129.8 8.6 %copy-start.2 = (f32[2,256]{1,0:T(2,128)S(1)}, f32[2,256]{1,0:T(2,128)}, u32[]{:S(2)}) copy-start(f32[2,256]{1,0:T(2,128)} %param.16) | copy-start | bytes 6148
  134.0 9.2 %all-to-all-start = ((f32[8,1,1536]{2,1,0:T(1,128)}), f32[8,1,1536]{2,1,0:T(1,128)S(1)}, u32[]{:S(2)}, u32[]{:S(2)}) async-start(f32[8,1,1536]{2,1,0:T(1,128)} %broadcast_in_dim.4), calls=%async_computation | async-start | bytes 98304 | tf_op jit(solution)/shard_map/all_to_all | solution.py:27
  138.4 131.2 %all-gather.15.cloned.1.call-start = ((), (), s32[]{:S(2)}) async-start(), calls=%async_computation.6 | async-start | bytes 3538944 | tf_op jit(solution)/shard_map/all_gather | solution.py:75
  205.7 1.0 copy-start
  207.8 96.4 %all-gather.21.cloned.1.call-start = ((), (), s32[]{:S(2)}) async-start(), calls=%async_computation.9 | async-start | bytes 1179648 | tf_op jit(solution)/shard_map/all_gather | solution.py:49
  235.4 37.5 %copy-start.5 = (bf16[2048,512]{1,0:T(8,128)(2,1)S(1)}, bf16[2048,512]{1,0:T(8,128)(2,1)}, u32[]{:S(2)}) copy-start(bf16[2048,512]{1,0:T(8,128)(2,1)} %all-gather.17.cloned.1.call-done) | copy-start | bytes 6291460
  269.6 3.3 copy-start.4
  273.9 4.0 %collective-permute-start.1 = (bf16[30,256]{1,0:T(8,128)(2,1)S(1)}, bf16[30,256]{1,0:T(8,128)(2,1)S(1)}, u32[]{:S(2)}, u32[]{:S(2)}) collective-permute-start(bf16[30,256]{1,0:T(8,128)(2,1)S(1)} %slice.610), channel_id=1, source_target_pairs={{0,8},{8,16},{16,24},{24,32},{32,40},{40,48},{48,56},{56,64},{64,7... | collective-permute-start | bytes 46088 | tf_op jit(solution)/shard_map/ppermute | solution.py:22
Sparse Core Ops, SparseCore 0:
  9.9 77.1 all-gather.12
  88.9 32.4 all-gather.10
  123.2 33.7 all-gather.18
  159.4 75.9 all-gather.16
  237.0 32.4 all-gather.14
  271.2 32.9 all-gather.20
where the time goes:
time: 363 us; the launch traced here: 362 us
  waiting for transfers between devices  177 us (49%)
  blocking collectives  124 us (34%)
  other arithmetic  14.7 us (4%)
  between operations  13.7 us (4%)
  matrix products  13.3 us (4%)
  starting transfers between devices  10.8 us (3%)
  local copies, waits for them, and re-layouts  7.75 us (2%)
    all_to_all x2, blocking collectives, sum_at_owner(): lax.all_to_all(tiles, axis, split_axis=0, concat_axis=0, tiled=True)  93.5 us
    all_gather x2, waiting for transfers between devices, sent_together(): whole = lax.all_gather(both, axis, axis=dim, tiled=True)  75.5 us
    all_gather x2, waiting for transfers between devices, body(): tokens = lax.all_gather(normed, 'tp', axis=0, tiled=True)  68.5 us
    all_gather x2, waiting for transfers between devices, whole_of(): nearer = lax.all_gather(shard, axes[-1], axis=dim, tiled=True)  27.6 us
    all_gather x2, blocking collectives, whole_of(): nearer = lax.all_gather(shard, axes[-1], axis=dim, tiled=True)  22.2 us
    all_to_all x1, blocking collectives, sent_to_all(): lax.all_to_all(jnp.broadcast_to(shard[None], (size, *shard.shape)), axis,...  8.63 us
  transfers between devices with their start and end apart: 9, of which 8 were waited for; matrix products, arithmetic and copies ran while one was open for 8% of the time, Pallas kernels for 0%

commit v1 on v0

--- a/solution.py
+++ b/solution.py
@@ -7,6 +7,28 @@
 SP = ("sp_0", "sp_1")
 SP_TP = ("sp_0", "sp_1", "tp")
 EPS = 1e-06
+
+
+def joined_along(parts, dim):
+    shape = list(parts.shape[1:])
+    shape[dim] *= parts.shape[0]
+    return jnp.moveaxis(parts, 0, dim).reshape(shape)
+
+
+def collect(shard, axis, dim):
+    size = lax.axis_size(axis)
+    pairs = [(i, (i + 1) % size) for i in range(size)]
+    back = [(b, a) for a, b in pairs]
+    lower, upper = ([], [])
+    for step in range(size - 1):
+        if step % 2 == 0:
+            lower.append(lax.ppermute(lower[-1] if lower else shard, axis, pairs))
+        else:
+            upper.append(lax.ppermute(upper[-1] if upper else shard, axis, back))
+    blocks = jnp.stack([*lower[::-1], shard, *upper])
+    shift = lax.axis_index(axis) - len(lower)
+    blocks = blocks[(jnp.arange(size) - shift) % size]
+    return joined_along(blocks, dim)
 
 
 def sent_together(arrays, axis, dim, along):
@@ -72,7 +94,7 @@
         xf = state.astype(jnp.float32)
         scale = lax.rsqrt(jnp.mean(xf * xf, axis=1, keepdims=True) + EPS)
         normed = (xf * scale * norm_gain[layer][None, :]).astype(jnp.bfloat16)
-        tokens = lax.all_gather(normed, "tp", axis=0, tiled=True)
+        tokens = collect(normed, "tp", 0)
         empty = jnp.zeros((tokens.shape[0], chans), jnp.float32)
 
         def add_both(totals, pieces, start, tokens=tokens):

time: 363 us -> 309 us (0.85)
  waiting for transfers between devices: 177 us -> 101 us
  starting transfers between devices: 10.8 us -> 57.5 us
  blocking collectives: 124 us -> 78.7 us
  local copies, waits for them, and re-layouts: 7.75 us -> 26.1 us
    all_gather x2 -> x0, waiting for transfers between devices: 68.5 us -> none  [body(): tokens = lax.all_gather(normed, 'tp', axis=0, tiled=True)]
    all_to_all x2 -> x1, blocking collectives: 93.5 us -> 47.2 us  [sum_at_owner(): lax.all_to_all(tiles, axis, split_axis=0, concat_axis=0, tiled=True)]
    all_gather x2, waiting for transfers between devices: 75.5 us -> 29.7 us  [sent_together(): whole = lax.all_gather(both, axis, axis=dim, tiled=True)]
    all_to_all x0 -> x1, waiting for transfers between devices: none -> 36 us  [sum_at_owner(): lax.all_to_all(tiles, axis, split_axis=0, concat_axis=0, tiled=True)]
    ppermute x0 -> x14, starting transfers between devices: none -> 32.3 us  [the longest x8 18.8 us: collect(): lower.append(lax.ppermute(lower[-1] if lower else shard, axis, pairs))]
    ppermute x0 -> x14, waiting for transfers between devices: none -> 18.1 us  [the longest x8 14.6 us: collect(): lower.append(lax.ppermute(lower[-1] if lower else shard, axis, pairs))]
    all_gather x2, waiting for transfers between devices: 27.6 us -> 12.1 us  [whole_of(): nearer = lax.all_gather(shard, axes[-1], axis=dim, tiled=True)]
    all_to_all x0 -> x1, starting transfers between devices: none -> 9.95 us  [sum_at_owner(): lax.all_to_all(tiles, axis, split_axis=0, concat_axis=0, tiled=True)]
  transfers between devices with their start and end apart: 9 -> 22, of which waited for: 8 -> 14; matrix products, arithmetic and copies ran while one was open for 8% -> 14% of each run, Pallas kernels for 0% -> 0%
where the time goes in v1:
time: 309 us; the launch traced here: 307 us
  waiting for transfers between devices  101 us (33%)
  blocking collectives  78.7 us (25%)
  starting transfers between devices  57.5 us (19%)
  local copies, waits for them, and re-layouts  26.1 us (8%)
  other arithmetic  14.9 us (5%)
  matrix products  14.9 us (5%)
  between operations  14.3 us (5%)
    all_to_all x1, blocking collectives, sum_at_owner(): lax.all_to_all(tiles, axis, split_axis=0, concat_axis=0, tiled=True)  47.2 us
    all_to_all x1, waiting for transfers between devices, sum_at_owner(): lax.all_to_all(tiles, axis, split_axis=0, concat_axis=0, tiled=True)  36 us
    all_gather x2, waiting for transfers between devices, sent_together(): whole = lax.all_gather(both, axis, axis=dim, tiled=True)  29.7 us
    all_gather x2, blocking collectives, whole_of(): nearer = lax.all_gather(shard, axes[-1], axis=dim, tiled=True)  21.6 us
    ppermute x8, starting transfers between devices, collect(): lower.append(lax.ppermute(lower[-1] if lower else shard, axis, pairs))  18.8 us
    ppermute x8, waiting for transfers between devices, collect(): lower.append(lax.ppermute(lower[-1] if lower else shard, axis, pairs))  14.6 us
    ppermute x6, starting transfers between devices, collect(): upper.append(lax.ppermute(upper[-1] if upper else shard, axis, back))  13.5 us
    all_gather x2, waiting for transfers between devices, whole_of(): nearer = lax.all_gather(shard, axes[-1], axis=dim, tiled=True)  12.1 us
  transfers between devices with their start and end apart: 22, of which 14 were waited for; matrix products, arithmetic and copies ran while one was open for 14% of the time, Pallas kernels for 0%

profile of v1, /device:TPU:1, one launch (start us, length us, event | category | flops | bytes accessed | tf_op | source)
XLA Modules:
  0.0 307.4 jit_solution(10079257578309725555)
XLA Ops:
  6.5 1.5 slice_bitcast_fusion
  8.7 1.2 fusion.14
  10.7 1.2 fusion.16
  11.9 2.6 collective-permute-start
  15.1 4.1 %collective-permute-done = bf16[96,2048]{1,0:T(8,128)(2,1)S(1)} collective-permute-done((bf16[96,2048]{1,0:T(8,128)(2,1)S(1)}, bf16[96,2048]{1,0:T(8,128)(2,1)S(1)}, u32[]{:S(2)}, u32[]{:S(2)}) %collective-permute-start) | collective-permute-done | bytes 393248 | tf_op jit(solution)/shard_map/ppermute | solution.py:25
  19.2 2.5 collective-permute-start.1
  21.7 1.4 fusion.109
  23.1 10.7 %all-gather = bf16[1,256,256]{1,2,0:T(8,128)(2,1)} all-gather(bf16[1,256,64]{1,2,0:T(8,128)(2,1)S(1)} %get-tuple-element.17), channel_id=2, replica_groups=mesh['sp_0'=8,'sp_1'=4,'tp'=8] {'sp_1'}, dimensions={2}, use_global_device_ids=true | all-gather | bytes 163840 | tf_op jit(solution)/shard_map/all_gather | solution.py:71
  34.5 2.6 collective-permute-start.2
  37.1 1.4 fusion.113
  38.5 1.5 fusion.112
  40.0 1.4 collective-permute-start.5
  41.8 2.5 collective-permute-start.3
  44.3 1.4 fusion.117
  45.7 1.5 fusion.111
  47.6 2.1 collective-permute-start.6
  52.1 2.7 collective-permute-done.6
  54.9 2.5 gather_fusion
  57.4 29.7 %all-gather.9.cloned.1.call-done = bf16[2048,512]{1,0:T(8,128)(2,1)} async-done(((bf16[64,512]{1,0:T(8,128)(2,1)}), bf16[2048,512]{1,0:T(8,128)(2,1)}) %all-gather.9.cloned.1.call-update) | async-done | bytes 2097168 | tf_op jit(solution)/shard_map/all_gather | solution.py:37
  87.1 3.3 %fusion.3 = f32[768,256]{1,0:T(8,128)S(1)} fusion(bf16[768,2048]{1,0:T(8,128)(2,1)} %bitcast.129, bf16[2048,512]{1,0:T(8,128)(2,1)} %all-gather.9.cloned.1.call-done), kind=kOutput, calls=%fused_computation.13 | convolution fusion | flops 805896192 | bytes 4980736 | tf_op jit(solution)/shard_map/dot_general | solution.py:103
  92.2 2.4 collective-permute-start.7
  95.8 3.5 %fusion.105 = (f32[768]{0:T(1024)S(1)}, f32[768]{0:T(1024)S(1)}, f32[768,256]{1,0:T(8,128)S(1)}) fusion(f32[798,256]{1,0:T(8,128)S(1)} %maximum_convert_fusion, f32[256]{0:T(256)S(1)} %bitcast.170, f32[256]{0:T(256)S(1)} %bitcast.171, f32[256]{0:T(256)S(1)} %bitcast.172, f32[256]{0:T(256)S(1)} %bitcast.173, f32[256]{0:T(256)S(1)} %bitcast.174, ...), kind=kLoop, calls=%fused_computation.224 | loop fusion | flops 12777984 | bytes 25204736 | tf_op jit(solution)/shard_map/reduce_sum | solution.py:116
  100.0 9.9 %all-to-all-start = ((f32[8,1,1536]{2,1,0:T(1,128)}), f32[8,1,1536]{2,1,0:T(1,128)S(1)}, u32[]{:S(2)}, u32[]{:S(2)}) async-start(f32[8,1,1536]{2,1,0:T(1,128)} %broadcast_in_dim.4), calls=%async_computation | async-start | bytes 98304 | tf_op jit(solution)/shard_map/all_to_all | solution.py:49
  110.5 4.2 %all-to-all-done = f32[8,1,1536]{2,1,0:T(1,128)S(1)} async-done(((f32[8,1,1536]{2,1,0:T(1,128)}), f32[8,1,1536]{2,1,0:T(1,128)S(1)}, u32[]{:S(2)}, u32[]{:S(2)}) %all-to-all-start) | async-done | bytes 49184 | tf_op jit(solution)/shard_map/all_to_all | solution.py:49
  114.8 9.3 %all-gather.13.cloned.1.call-done = bf16[1,256,2048]{1,2,0:T(8,128)(2,1)} async-done(((bf16[1,256,256]{1,2,0:T(8,128)(2,1)}), bf16[1,256,2048]{1,2,0:T(8,128)(2,1)}) %all-gather.13.cloned.1.call-update) | async-done | bytes 1048592 | tf_op jit(solution)/shard_map/all_gather | solution.py:71
  124.1 4.0 %convolution_convert_fusion.1 = bf16[768,2048]{1,0:T(8,128)(2,1)} fusion(bf16[1,256,2048]{1,2,0:T(8,128)(2,1)} %all-gather.13.cloned.1.call-done, f32[768,256]{1,0:T(8,128)S(1)} %get-tuple-element.12, f32[256]{0:T(256)S(1)} %bitcast.203, f32[256]{0:T(256)S(1)} %bitcast.202, f32[768]{0:T(1024)S(1)} %get-tuple-element.86, f32[768]{0:T(1024)S(1)} %get-tuple-element.85), kind=kOutput, calls=%fused_computation.5 | convolution fusion | flops 808648704 | bytes 4988928 | tf_op jit(solution)/shard_map/dot_general | solution.py:126
  128.1 10.0 %all-to-all-start.1 = ((bf16[8,96,2048]{2,1,0:T(8,128)(2,1)}), bf16[8,96,2048]{2,1,0:T(8,128)(2,1)S(1)}, u32[]{:S(2)}, u32[]{:S(2)}) async-start(bf16[8,96,2048]{2,1,0:T(8,128)(2,1)} %bitcast.126), calls=%async_computation.1 | async-start | bytes 6291456 | tf_op jit(solution)/shard_map/all_to_all | solution.py:83
  138.1 1.4 pad_maximum_fusion.1
  139.5 36.0 %all-to-all-done.1 = bf16[8,96,2048]{2,1,0:T(8,128)(2,1)S(1)} async-done(((bf16[8,96,2048]{2,1,0:T(8,128)(2,1)}), bf16[8,96,2048]{2,1,0:T(8,128)(2,1)S(1)}, u32[]{:S(2)}, u32[]{:S(2)}) %all-to-all-start.1) | async-done | bytes 3145760 | tf_op jit(solution)/shard_map/all_to_all | solution.py:83
  176.5 1.2 collective-permute-start.8
  177.6 4.7 %collective-permute-done.8 = bf16[96,2048]{1,0:T(8,128)(2,1)S(1)} collective-permute-done((bf16[96,2048]{1,0:T(8,128)(2,1)S(1)}, bf16[96,2048]{1,0:T(8,128)(2,1)S(1)}, u32[]{:S(2)}, u32[]{:S(2)}) %collective-permute-start.8) | collective-permute-done | bytes 393248 | tf_op jit(solution)/shard_map/ppermute | solution.py:25
  183.1 2.5 collective-permute-start.9
  186.6 3.7 %collective-permute-done.9 = bf16[96,2048]{1,0:T(8,128)(2,1)S(1)} collective-permute-done((bf16[96,2048]{1,0:T(8,128)(2,1)S(1)}, bf16[96,2048]{1,0:T(8,128)(2,1)S(1)}, u32[]{:S(2)}, u32[]{:S(2)}) %collective-permute-start.9) | collective-permute-done | bytes 393248 | tf_op jit(solution)/shard_map/ppermute | solution.py:25
  190.3 2.5 collective-permute-start.10
  193.2 2.6 collective-permute-start.13
  195.8 1.7 collective-permute-done.10
  197.5 2.5 collective-permute-start.11
  200.0 10.9 %all-gather.2 = bf16[1,256,256]{1,2,0:T(8,128)(2,1)} all-gather(bf16[1,256,64]{1,2,0:T(8,128)(2,1)S(1)} %copy-done.12), channel_id=4, replica_groups=mesh['sp_0'=8,'sp_1'=4,'tp'=8] {'sp_1'}, dimensions={2}, use_global_device_ids=true | all-gather | bytes 163840 | tf_op jit(solution)/shard_map/all_gather | solution.py:71
  210.9 5.7 %collective-permute-start.14 = (bf16[96,2048]{1,0:T(8,128)(2,1)}, bf16[96,2048]{1,0:T(8,128)(2,1)S(1)}, u32[]{:S(2)}, u32[]{:S(2)}) collective-permute-start(bf16[96,2048]{1,0:T(8,128)(2,1)} %collective-permute-done.13), channel_id=1, source_target_pairs={{1,0},{2,1},{3,2},{4,3},{5,4},{6,5},{7,6},{0,7},{9,8},{10,9},{11,1... | collective-permute-start | bytes 1179656 | tf_op jit(solution)/shard_map/ppermute | solution.py:27
  216.7 1.1 bitcast_dynamic-update-slice_fusion.7
  222.1 2.5 gather_fusion.1
  224.6 3.3 %fusion.5 = f32[768,256]{1,0:T(8,128)S(1)} fusion(bf16[768,2048]{1,0:T(8,128)(2,1)} %bitcast.127, bf16[2048,512]{1,0:T(8,128)(2,1)} %all-gather.11.cloned.1.call-done), kind=kOutput, calls=%fused_computation.15 | convolution fusion | flops 805896192 | bytes 4980736 | tf_op jit(solution)/shard_map/dot_general | solution.py:103
  229.6 2.9 collective-permute-start.15
  233.7 3.5 %fusion.104 = (f32[768]{0:T(1024)S(1)}, f32[768]{0:T(1024)S(1)}, f32[768,256]{1,0:T(8,128)S(1)}) fusion(f32[798,256]{1,0:T(8,128)S(1)} %maximum_convert_fusion.1, f32[256]{0:T(256)S(1)} %bitcast.136, f32[256]{0:T(256)S(1)} %bitcast.137, f32[256]{0:T(256)S(1)} %bitcast.180, f32[256]{0:T(256)S(1)} %bitcast.181, f32[256]{0:T(256)S(1)} %bitcast.182, ...), kind=kLoop, calls=%fused_computation.223 | loop fusion | flops 12777984 | bytes 25204736 | tf_op jit(solution)/shard_map/reduce_sum | solution.py:116
  237.2 9.9 %all_to_all.22 = f32[8,1,1536]{2,1,0:T(1,128)S(1)} all-to-all(f32[8,1,1536]{2,1,0:T(1,128)S(1)} %broadcast_in_dim.5), channel_id=1, replica_groups=mesh['sp_0'=8,'sp_1'=4,'tp'=8] {'tp'}, dimensions={0} | all-to-all | bytes 98304 | tf_op jit(solution)/shard_map/all_to_all | solution.py:49
  247.2 2.8 all-gather.15.cloned.1.call-done
  250.0 2.3 convolution_convert_fusion
  252.3 47.2 %all_to_all.23 = bf16[8,96,2048]{2,1,0:T(8,128)(2,1)S(1)} all-to-all(bf16[8,96,2048]{2,1,0:T(8,128)(2,1)S(1)} %bitcast.131), channel_id=1, replica_groups=mesh['sp_0'=8,'sp_1'=4,'tp'=8] {'tp'}, dimensions={0} | all-to-all | bytes 6291456 | tf_op jit(solution)/shard_map/all_to_all | solution.py:83
  (195 shorter events, 21.5 us)
Async XLA Ops:
  6.5 45.3 %copy-start = (bf16[96,2048]{1,0:T(8,128)(2,1)S(1)}, bf16[96,2048]{1,0:T(8,128)(2,1)}, u32[]{:S(2)}) copy-start(bf16[96,2048]{1,0:T(8,128)(2,1)} %param.9) | copy-start | bytes 1179652
  6.5 80.5 %all-gather.9.cloned.1.call-start = ((), (), s32[]{:S(2)}) async-start(), calls=%async_computation.4 | async-start | bytes 2162688 | tf_op jit(solution)/shard_map/all_gather | solution.py:37
  8.7 115.4 %all-gather.13.cloned.1.call-start = ((), (), s32[]{:S(2)}) async-start(), calls=%async_computation.6 | async-start | bytes 1179648 | tf_op jit(solution)/shard_map/all_gather | solution.py:71
  9.9 9.3 %copy-start.60 = (f32[96]{0:T(128)}, f32[96]{0:T(128)S(1)}, u32[]{:S(2)}) copy-start(f32[96]{0:T(128)S(1)} %add_rsqrt_fusion.1) | copy-start | bytes 1156
  11.9 7.3 %collective-permute-start = (bf16[96,2048]{1,0:T(8,128)(2,1)S(1)}, bf16[96,2048]{1,0:T(8,128)(2,1)S(1)}, u32[]{:S(2)}, u32[]{:S(2)}) collective-permute-start(bf16[96,2048]{1,0:T(8,128)(2,1)S(1)} %fusion.16), channel_id=1, source_target_pairs={{0,1},{1,2},{2,3},{3,4},{4,5},{5,6},{6,7},{7,0},{8,9},{9,10},{10,1... | collective-permute-start | bytes 1179656 | tf_op jit(solution)/shard_map/ppermute | solution.py:25
  14.5 25.5 %collective-permute-start.4 = (bf16[96,2048]{1,0:T(8,128)(2,1)S(1)}, bf16[96,2048]{1,0:T(8,128)(2,1)S(1)}, u32[]{:S(2)}, u32[]{:S(2)}) collective-permute-start(bf16[96,2048]{1,0:T(8,128)(2,1)S(1)} %fusion.16), channel_id=1, source_target_pairs={{1,0},{2,1},{3,2},{4,3},{5,4},{6,5},{7,6},{0,7},{9,8},{10,9},{11,1... | collective-permute-start | bytes 1179656 | tf_op jit(solution)/shard_map/ppermute | solution.py:27
  19.2 30.5 %copy-start.5 = (bf16[96,2048]{1,0:T(8,128)(2,1)}, bf16[96,2048]{1,0:T(8,128)(2,1)S(1)}, u32[]{:S(2)}) copy-start(bf16[96,2048]{1,0:T(8,128)(2,1)S(1)} %collective-permute-done) | copy-start | bytes 1179652
  19.2 15.2 %collective-permute-start.1 = (bf16[96,2048]{1,0:T(8,128)(2,1)S(1)}, bf16[96,2048]{1,0:T(8,128)(2,1)S(1)}, u32[]{:S(2)}, u32[]{:S(2)}) collective-permute-start(bf16[96,2048]{1,0:T(8,128)(2,1)S(1)} %collective-permute-done), channel_id=1, source_target_pairs={{0,1},{1,2},{2,3},{3,4},{4,5},{5,6},{6,7},{7,0},{8,9},{9,10},{10,1... | collective-permute-start | bytes 1179656 | tf_op jit(solution)/shard_map/ppermute | solution.py:25
  33.8 18.0 %copy-start.61 = (f32[96]{0:T(128)S(1)}, f32[96]{0:T(128)}, u32[]{:S(2)}) copy-start(f32[96]{0:T(128)} %copy-done.60) | copy-start | bytes 1156
  34.5 15.2 %copy-start.6 = (bf16[96,2048]{1,0:T(8,128)(2,1)}, bf16[96,2048]{1,0:T(8,128)(2,1)S(1)}, u32[]{:S(2)}) copy-start(bf16[96,2048]{1,0:T(8,128)(2,1)S(1)} %collective-permute-done.1) | copy-start | bytes 1179652
  34.5 7.4 %collective-permute-start.2 = (bf16[96,2048]{1,0:T(8,128)(2,1)S(1)}, bf16[96,2048]{1,0:T(8,128)(2,1)S(1)}, u32[]{:S(2)}, u32[]{:S(2)}) collective-permute-start(bf16[96,2048]{1,0:T(8,128)(2,1)S(1)} %collective-permute-done.1), channel_id=1, source_target_pairs={{0,1},{1,2},{2,3},{3,4},{4,5},{5,6},{6,7},{7,0},{8,9},{9,10},{10,1... | collective-permute-start | bytes 1179656 | tf_op jit(solution)/shard_map/ppermute | solution.py:25
  40.0 9.7 %copy-start.3 = (bf16[96,2048]{1,0:T(8,128)(2,1)}, bf16[96,2048]{1,0:T(8,128)(2,1)S(1)}, u32[]{:S(2)}) copy-start(bf16[96,2048]{1,0:T(8,128)(2,1)S(1)} %collective-permute-done.4) | copy-start | bytes 1179652
  40.0 7.6 %collective-permute-start.5 = (bf16[96,2048]{1,0:T(8,128)(2,1)S(1)}, bf16[96,2048]{1,0:T(8,128)(2,1)S(1)}, u32[]{:S(2)}, u32[]{:S(2)}) collective-permute-start(bf16[96,2048]{1,0:T(8,128)(2,1)S(1)} %collective-permute-done.4), channel_id=1, source_target_pairs={{1,0},{2,1},{3,2},{4,3},{5,4},{6,5},{7,6},{0,7},{9,8},{10,9},{11,1... | collective-permute-start | bytes 1179656 | tf_op jit(solution)/shard_map/ppermute | solution.py:27
  41.8 7.9 %collective-permute-start.3 = (bf16[96,2048]{1,0:T(8,128)(2,1)S(1)}, bf16[96,2048]{1,0:T(8,128)(2,1)S(1)}, u32[]{:S(2)}, u32[]{:S(2)}) collective-permute-start(bf16[96,2048]{1,0:T(8,128)(2,1)S(1)} %collective-permute-done.2), channel_id=1, source_target_pairs={{0,1},{1,2},{2,3},{3,4},{4,5},{5,6},{6,7},{7,0},{8,9},{9,10},{10,1... | collective-permute-start | bytes 1179656 | tf_op jit(solution)/shard_map/ppermute | solution.py:25
  47.6 7.2 %collective-permute-start.6 = (bf16[96,2048]{1,0:T(8,128)(2,1)S(1)}, bf16[96,2048]{1,0:T(8,128)(2,1)S(1)}, u32[]{:S(2)}, u32[]{:S(2)}) collective-permute-start(bf16[96,2048]{1,0:T(8,128)(2,1)S(1)} %collective-permute-done.5), channel_id=1, source_target_pairs={{1,0},{2,1},{3,2},{4,3},{5,4},{6,5},{7,6},{0,7},{9,8},{10,9},{11,1... | collective-permute-start | bytes 1179656 | tf_op jit(solution)/shard_map/ppermute | solution.py:27
  90.9 4.6 %copy-start.28 = (f32[1,1,256]{2,0,1:T(1,128)S(1)}, f32[1,1,256]{2,0,1:T(1,128)}, u32[]{:S(2)}) copy-start(f32[1,1,256]{2,0,1:T(1,128)} %get-tuple-element.80) | copy-start | bytes 3076
  90.9 4.6 %copy-start.29 = (f32[1,1,256]{2,0,1:T(1,128)S(1)}, f32[1,1,256]{2,0,1:T(1,128)}, u32[]{:S(2)}) copy-start(f32[1,1,256]{2,0,1:T(1,128)} %get-tuple-element.58) | copy-start | bytes 3076
  92.2 3.2 %collective-permute-start.7 = (bf16[30,256]{1,0:T(8,128)(2,1)S(1)}, bf16[30,256]{1,0:T(8,128)(2,1)S(1)}, u32[]{:S(2)}, u32[]{:S(2)}) collective-permute-start(bf16[30,256]{1,0:T(8,128)(2,1)S(1)} %slice.580), channel_id=1, source_target_pairs={{0,8},{8,16},{16,24},{24,32},{32,40},{40,48},{48,56},{56,64},{64,7... | collective-permute-start | bytes 46088 | tf_op jit(solution)/shard_map/ppermute | solution.py:44
  95.8 14.1 %copy-start.59 = (f32[2,256]{1,0:T(2,128)S(1)}, f32[2,256]{1,0:T(2,128)}, u32[]{:S(2)}) copy-start(f32[2,256]{1,0:T(2,128)} %param.16) | copy-start | bytes 6148
  100.0 14.7 %all-to-all-start = ((f32[8,1,1536]{2,1,0:T(1,128)}), f32[8,1,1536]{2,1,0:T(1,128)S(1)}, u32[]{:S(2)}, u32[]{:S(2)}) async-start(f32[8,1,1536]{2,1,0:T(1,128)} %broadcast_in_dim.4), calls=%async_computation | async-start | bytes 98304 | tf_op jit(solution)/shard_map/all_to_all | solution.py:49
  128.1 47.4 %all-to-all-start.1 = ((bf16[8,96,2048]{2,1,0:T(8,128)(2,1)}), bf16[8,96,2048]{2,1,0:T(8,128)(2,1)S(1)}, u32[]{:S(2)}, u32[]{:S(2)}) async-start(bf16[8,96,2048]{2,1,0:T(8,128)(2,1)} %bitcast.126), calls=%async_computation.1 | async-start | bytes 6291456 | tf_op jit(solution)/shard_map/all_to_all | solution.py:83
  138.1 86.6 %all-gather.11.cloned.1.call-start = ((), (), s32[]{:S(2)}) async-start(), calls=%async_computation.5 | async-start | bytes 2162688 | tf_op jit(solution)/shard_map/all_gather | solution.py:37
  139.5 110.5 %all-gather.15.cloned.1.call-start = ((), (), s32[]{:S(2)}) async-start(), calls=%async_computation.7 | async-start | bytes 1179648 | tf_op jit(solution)/shard_map/all_gather | solution.py:71
  175.5 24.5 %copy-start.12 = (bf16[1,256,64]{1,2,0:T(8,128)(2,1)S(1)}, bf16[1,256,64]{1,2,0:T(8,128)(2,1)}, u32[]{:S(2)}) copy-start(bf16[1,256,64]{1,2,0:T(8,128)(2,1)} %get-tuple-element.18) | copy-start | bytes 98308
  176.5 5.9 %collective-permute-start.8 = (bf16[96,2048]{1,0:T(8,128)(2,1)S(1)}, bf16[96,2048]{1,0:T(8,128)(2,1)S(1)}, u32[]{:S(2)}, u32[]{:S(2)}) collective-permute-start(bf16[96,2048]{1,0:T(8,128)(2,1)S(1)} %fusion.20), channel_id=1, source_target_pairs={{0,1},{1,2},{2,3},{3,4},{4,5},{5,6},{6,7},{7,0},{8,9},{9,10},{10,1... | collective-permute-start | bytes 1179656 | tf_op jit(solution)/shard_map/ppermute | solution.py:25
  183.1 7.2 %collective-permute-start.9 = (bf16[96,2048]{1,0:T(8,128)(2,1)S(1)}, bf16[96,2048]{1,0:T(8,128)(2,1)S(1)}, u32[]{:S(2)}, u32[]{:S(2)}) collective-permute-start(bf16[96,2048]{1,0:T(8,128)(2,1)S(1)} %collective-permute-done.8), channel_id=1, source_target_pairs={{0,1},{1,2},{2,3},{3,4},{4,5},{5,6},{6,7},{7,0},{8,9},{9,10},{10,1... | collective-permute-start | bytes 1179656 | tf_op jit(solution)/shard_map/ppermute | solution.py:25
  185.6 7.6 %collective-permute-start.12 = (bf16[96,2048]{1,0:T(8,128)(2,1)S(1)}, bf16[96,2048]{1,0:T(8,128)(2,1)S(1)}, u32[]{:S(2)}, u32[]{:S(2)}) collective-permute-start(bf16[96,2048]{1,0:T(8,128)(2,1)S(1)} %fusion.20), channel_id=1, source_target_pairs={{1,0},{2,1},{3,2},{4,3},{5,4},{6,5},{7,6},{0,7},{9,8},{10,9},{11,1... | collective-permute-start | bytes 1179656 | tf_op jit(solution)/shard_map/ppermute | solution.py:27
  190.3 7.2 %collective-permute-start.10 = (bf16[96,2048]{1,0:T(8,128)(2,1)S(1)}, bf16[96,2048]{1,0:T(8,128)(2,1)S(1)}, u32[]{:S(2)}, u32[]{:S(2)}) collective-permute-start(bf16[96,2048]{1,0:T(8,128)(2,1)S(1)} %collective-permute-done.9), channel_id=1, source_target_pairs={{0,1},{1,2},{2,3},{3,4},{4,5},{5,6},{6,7},{7,0},{8,9},{9,10},{10,1... | collective-permute-start | bytes 1179656 | tf_op jit(solution)/shard_map/ppermute | solution.py:25
  193.2 23.5 %copy-start.8 = (bf16[96,2048]{1,0:T(8,128)(2,1)}, bf16[96,2048]{1,0:T(8,128)(2,1)S(1)}, u32[]{:S(2)}) copy-start(bf16[96,2048]{1,0:T(8,128)(2,1)S(1)} %collective-permute-done.12) | copy-start | bytes 1179652
  193.2 17.7 %collective-permute-start.13 = (bf16[96,2048]{1,0:T(8,128)(2,1)S(1)}, bf16[96,2048]{1,0:T(8,128)(2,1)}, u32[]{:S(2)}, u32[]{:S(2)}) collective-permute-start(bf16[96,2048]{1,0:T(8,128)(2,1)S(1)} %collective-permute-done.12), channel_id=1, source_target_pairs={{1,0},{2,1},{3,2},{4,3},{5,4},{6,5},{7,6},{0,7},{9,8},{10,9},{11,1... | collective-permute-start | bytes 1179656 | tf_op jit(solution)/shard_map/ppermute | solution.py:27
  197.5 19.2 %copy-start.11 = (bf16[96,2048]{1,0:T(8,128)(2,1)}, bf16[96,2048]{1,0:T(8,128)(2,1)S(1)}, u32[]{:S(2)}) copy-start(bf16[96,2048]{1,0:T(8,128)(2,1)S(1)} %collective-permute-done.10) | copy-start | bytes 1179652
  197.5 19.2 %collective-permute-start.11 = (bf16[96,2048]{1,0:T(8,128)(2,1)S(1)}, bf16[96,2048]{1,0:T(8,128)(2,1)}, u32[]{:S(2)}, u32[]{:S(2)}) collective-permute-start(bf16[96,2048]{1,0:T(8,128)(2,1)S(1)} %collective-permute-done.10), channel_id=1, source_target_pairs={{0,1},{1,2},{2,3},{3,4},{4,5},{5,6},{6,7},{7,0},{8,9},{9,10},{10,1... | collective-permute-start | bytes 1179656 | tf_op jit(solution)/shard_map/ppermute | solution.py:25
  210.9 11.1 %collective-permute-start.14 = (bf16[96,2048]{1,0:T(8,128)(2,1)}, bf16[96,2048]{1,0:T(8,128)(2,1)S(1)}, u32[]{:S(2)}, u32[]{:S(2)}) collective-permute-start(bf16[96,2048]{1,0:T(8,128)(2,1)} %collective-permute-done.13), channel_id=1, source_target_pairs={{1,0},{2,1},{3,2},{4,3},{5,4},{6,5},{7,6},{0,7},{9,8},{10,9},{11,1... | collective-permute-start | bytes 1179656 | tf_op jit(solution)/shard_map/ppermute | solution.py:27
  228.5 5.0 %copy-start.13 = (f32[1,1,256]{2,0,1:T(1,128)S(1)}, f32[1,1,256]{2,0,1:T(1,128)}, u32[]{:S(2)}) copy-start(f32[1,1,256]{2,0,1:T(1,128)} %get-tuple-element.76) | copy-start | bytes 3076
  228.5 5.0 %copy-start.14 = (f32[1,1,256]{2,0,1:T(1,128)S(1)}, f32[1,1,256]{2,0,1:T(1,128)}, u32[]{:S(2)}) copy-start(f32[1,1,256]{2,0,1:T(1,128)} %get-tuple-element.57) | copy-start | bytes 3076
  228.5 5.0 %copy-start.15 = (f32[1,1,256]{2,0,1:T(1,128)S(1)}, f32[1,1,256]{2,0,1:T(1,128)}, u32[]{:S(2)}) copy-start(f32[1,1,256]{2,0,1:T(1,128)} %get-tuple-element.38) | copy-start | bytes 3076
  228.5 5.1 %copy-start.16 = (f32[1,1,256]{2,0,1:T(1,128)S(1)}, f32[1,1,256]{2,0,1:T(1,128)}, u32[]{:S(2)}) copy-start(f32[1,1,256]{2,0,1:T(1,128)} %get-tuple-element.39) | copy-start | bytes 3076
  228.5 5.1 %copy-start.17 = (f32[1,1,256]{2,0,1:T(1,128)S(1)}, f32[1,1,256]{2,0,1:T(1,128)}, u32[]{:S(2)}) copy-start(f32[1,1,256]{2,0,1:T(1,128)} %get-tuple-element.40) | copy-start | bytes 3076
  228.5 5.1 %copy-start.18 = (f32[1,1,256]{2,0,1:T(1,128)S(1)}, f32[1,1,256]{2,0,1:T(1,128)}, u32[]{:S(2)}) copy-start(f32[1,1,256]{2,0,1:T(1,128)} %get-tuple-element.41) | copy-start | bytes 3076
  228.5 5.1 %copy-start.19 = (f32[1,1,256]{2,0,1:T(1,128)S(1)}, f32[1,1,256]{2,0,1:T(1,128)}, u32[]{:S(2)}) copy-start(f32[1,1,256]{2,0,1:T(1,128)} %get-tuple-element.42) | copy-start | bytes 3076
  228.5 5.1 %copy-start.20 = (f32[1,1,256]{2,0,1:T(1,128)S(1)}, f32[1,1,256]{2,0,1:T(1,128)}, u32[]{:S(2)}) copy-start(f32[1,1,256]{2,0,1:T(1,128)} %get-tuple-element.43) | copy-start | bytes 3076
  228.5 5.1 %copy-start.21 = (f32[1,1,256]{2,0,1:T(1,128)S(1)}, f32[1,1,256]{2,0,1:T(1,128)}, u32[]{:S(2)}) copy-start(f32[1,1,256]{2,0,1:T(1,128)} %get-tuple-element.44) | copy-start | bytes 3076
  228.5 5.1 %copy-start.22 = (f32[1,1,256]{2,0,1:T(1,128)S(1)}, f32[1,1,256]{2,0,1:T(1,128)}, u32[]{:S(2)}) copy-start(f32[1,1,256]{2,0,1:T(1,128)} %get-tuple-element.45) | copy-start | bytes 3076
  228.6 5.1 %copy-start.23 = (f32[1,1,256]{2,0,1:T(1,128)S(1)}, f32[1,1,256]{2,0,1:T(1,128)}, u32[]{:S(2)}) copy-start(f32[1,1,256]{2,0,1:T(1,128)} %get-tuple-element.46) | copy-start | bytes 3076
  228.6 5.1 %copy-start.24 = (f32[1,1,256]{2,0,1:T(1,128)S(1)}, f32[1,1,256]{2,0,1:T(1,128)}, u32[]{:S(2)}) copy-start(f32[1,1,256]{2,0,1:T(1,128)} %get-tuple-element.47) | copy-start | bytes 3076
  228.6 5.1 %copy-start.56 = (f32[1,256]{1,0:T(1,128)S(1)}, f32[1,256]{1,0:T(1,128)}, u32[]{:S(2)}) copy-start(f32[1,256]{1,0:T(1,128)} %get-tuple-element.91) | copy-start | bytes 3076
  229.6 3.8 %collective-permute-start.15 = (bf16[30,256]{1,0:T(8,128)(2,1)S(1)}, bf16[30,256]{1,0:T(8,128)(2,1)S(1)}, u32[]{:S(2)}, u32[]{:S(2)}) collective-permute-start(bf16[30,256]{1,0:T(8,128)(2,1)S(1)} %slice.614), channel_id=1, source_target_pairs={{0,8},{8,16},{16,24},{24,32},{32,40},{40,48},{48,56},{56,64},{64,7... | collective-permute-start | bytes 46088 | tf_op jit(solution)/shard_map/ppermute | solution.py:44
  233.7 16.3 %copy-start.62 = (f32[1,256]{1,0:T(1,128)S(1)}, f32[1,256]{1,0:T(1,128)}, u32[]{:S(2)}) copy-start(f32[1,256]{1,0:T(1,128)} %get-tuple-element.89) | copy-start | bytes 3076
  (39 other events, 167.7 us)
Sparse Core Ops, SparseCore 0:
  9.9 77.1 all-gather.8
  88.9 35.2 all-gather.12
  141.4 71.6 all-gather.10
  214.7 35.1 all-gather.14
